TPU v7x, 128 devices: a whole 4x4x4 slice. The times are simulated.
128 devices in a mesh: sp: 16 (over z, y), tp: 8 (over x, core).
Axes of the slice: x: 4, y: 4, z: 4, core: 2. Of those that a mesh axis runs over, the one named last changes fastest.
Arguments:
- residual_in: bfloat16 [12288, 2048], P('sp', 'tp'), may hold values from -11 to 11
- queries: bfloat16 [12288, 1024], P('sp', 'tp'), may hold values from -6 to 6
- keys: bfloat16 [12288, 256], P('sp'), may hold values from -6 to 6
- values: bfloat16 [12288, 256], P('sp'), may hold values from -6 to 6
- query_gain: float32 [128], replicated, may hold values from 1.5 to 5
- key_norm_gain: float32 [128], replicated, may hold values from 1.5 to 5
- out_weight: bfloat16 [1024, 2048], P('tp'), may hold values from -0.1875 to 0.1875
- mlp_gain: float32 [2048], replicated, may hold values from 0.1 to 1.9
- gate_weight: bfloat16 [2048, 5632], P('sp', 'tp'), may hold values from -0.125 to 0.125
- up_weight: bfloat16 [2048, 5632], P('sp', 'tp'), may hold values from -0.125 to 0.125
- down_weight: bfloat16 [5632, 2048], P('tp', 'sp'), may hold values from -0.15625 to 0.15625
Outputs:
- layer_out: bfloat16 [12288, 2048], P('sp', 'tp')
All inputs are finite; a program needn't handle non-finite values.
Results may differ from a plain program's by a relative error of at most 0.012.
The roundings to bfloat16 on the way count: a program that leaves them out, or rounds other values in their place, can miss the bound.
Values may be sent and summed in bfloat16 or wider, within the bound.
A program may use at most 64 MiB of HBM per device.

v0:
```python
import jax
import jax.numpy as jnp
from jax import lax
from jax.sharding import PartitionSpec as P

D = 2048
HEAD_SIZE = 128
QUERY_HEADS = 8
KEY_VALUE_HEADS = 2
GRID = 64
eps = 1e-06
rotary_base = 10000.0


def sent_together(arrays, axis, dim, along):
    ends, at = ([], 0)
    for a in arrays[:-1]:
        at += a.shape[along]
        ends.append(at)
    both = jnp.concatenate(arrays, axis=along)
    return tuple(jnp.split(lax.all_gather(both, axis, axis=dim, tiled=True), ends, axis=along))


def laid_out(tiles, dim):
    tiles = jnp.moveaxis(tiles, 0, dim)
    lengths = tiles.shape
    return tiles.reshape(*lengths[:dim], lengths[dim] * lengths[dim + 1], *lengths[dim + 2 :])


def sent_to_all(x, axis):
    size = lax.axis_size(axis)
    return lax.all_to_all(jnp.broadcast_to(x[None], (size, *x.shape)), axis, 0, 0, tiled=True)


def gathered_copies(x, axis, dim):
    return laid_out(sent_to_all(x, axis), dim)


def taken_together(x, axis):
    everything = sent_to_all(x, axis)
    return jnp.sum(everything, axis=0)


def in_blocks(x, dim, size):
    lengths = x.shape
    tiles = x.reshape(*lengths[:dim], size, lengths[dim] // size, *lengths[dim + 1 :])
    return jnp.moveaxis(tiles, dim, 0)


def summed_on_arrival(x, axis, dim):
    tiles = in_blocks(x, dim, lax.axis_size(axis))
    arrived = lax.all_to_all(tiles, axis, split_axis=0, concat_axis=0, tiled=True)
    return arrived.astype(jnp.float32).sum(axis=0)


def apply_rotary(vectors, grid_positions):
    half_size = vectors.shape[-1] // 2
    frequency = rotary_base ** (-jnp.arange(0, half_size, 2, dtype=jnp.float32) / half_size)
    grid_row = (grid_positions // GRID).astype(jnp.float32)
    grid_col = (grid_positions % GRID).astype(jnp.float32)
    angles = jnp.concatenate(
        [grid_row[:, None] * frequency, grid_col[:, None] * frequency], axis=-1
    )[:, None, :]
    cosine_table = jnp.cos(angles)
    sine_table = jnp.sin(angles)
    first_half = vectors[..., :half_size]
    second_half = vectors[..., half_size:]
    return jnp.concatenate(
        [
            first_half * cosine_table - second_half * sine_table,
            first_half * sine_table + second_half * cosine_table,
        ],
        axis=-1,
    )


def per_head_norm(vectors, gain):
    return vectors * lax.rsqrt(jnp.mean(vectors * vectors, axis=-1, keepdims=True) + eps) * gain


def on_device(
    residual_in,
    queries,
    keys,
    values,
    query_gain,
    key_norm_gain,
    out_weight,
    mlp_gain,
    gate_weight,
    up_weight,
    down_weight,
):
    local_rows = residual_in.shape[0]
    local_heads = queries.shape[1] // HEAD_SIZE
    queries_per_group = QUERY_HEADS // KEY_VALUE_HEADS
    tp_index = lax.axis_index("tp")
    tp_count = lax.axis_size("tp")
    grid_positions = lax.axis_index("sp") * local_rows + jnp.arange(local_rows, dtype=jnp.int32)
    weight_cols = lax.all_to_all(out_weight, "tp", split_axis=1, concat_axis=0, tiled=True)
    query_rows = apply_rotary(
        per_head_norm(
            queries.astype(jnp.float32).reshape(local_rows, local_heads, HEAD_SIZE), query_gain
        ),
        grid_positions,
    ).astype(jnp.bfloat16)
    query_matrix = jnp.transpose(query_rows, (1, 0, 2)).reshape(local_heads * local_rows, HEAD_SIZE)
    shared = tp_index * local_heads // queries_per_group
    own_keys = lax.dynamic_slice_in_dim(keys, shared * HEAD_SIZE, HEAD_SIZE, 1)
    own_values = lax.dynamic_slice_in_dim(values, shared * HEAD_SIZE, HEAD_SIZE, 1)
    key_matrix = apply_rotary(
        per_head_norm(own_keys.astype(jnp.float32)[:, None, :], key_norm_gain), grid_positions
    )[:, 0, :].astype(jnp.bfloat16)
    score_scale = HEAD_SIZE ** (-0.5)
    query_count = local_heads * local_rows
    start_state = (
        jnp.full((query_count,), -1e30, jnp.float32),
        jnp.zeros((query_count,), jnp.float32),
        jnp.zeros((query_count, HEAD_SIZE), jnp.float32),
    )
    key_piece, value_piece = sent_together((key_matrix, own_values), "sp", 0, 1)
    piece_rows = key_piece.shape[0]
    block_count = -(-piece_rows // 2048)
    while piece_rows % block_count:
        block_count += 1
    block_width = piece_rows // block_count

    def one_block(block_index, state_inner):
        running_max, running_sum, weighted = state_inner
        block_keys = lax.dynamic_slice_in_dim(key_piece, block_index * block_width, block_width, 0)
        block_values = lax.dynamic_slice_in_dim(
            value_piece, block_index * block_width, block_width, 0
        )
        scores = (
            jnp.dot(query_matrix, block_keys.T, preferred_element_type=jnp.float32) * score_scale
        )
        new_max = jnp.maximum(running_max, jnp.max(scores, axis=1))
        factor = jnp.exp(running_max - new_max)
        weights = jnp.exp(scores - new_max[:, None])
        running_sum = running_sum * factor + jnp.sum(weights, axis=1)
        weighted = weighted * factor[:, None] + jnp.dot(
            weights.astype(jnp.bfloat16), block_values, preferred_element_type=jnp.float32
        )
        return (new_max, running_sum, weighted)

    running_max, running_sum, weighted = lax.fori_loop(0, block_count, one_block, start_state)
    attended = (weighted / running_sum[:, None]).astype(jnp.bfloat16)
    attended = jnp.transpose(
        attended.reshape(local_heads, local_rows, HEAD_SIZE), (1, 0, 2)
    ).reshape(local_rows, local_heads * HEAD_SIZE)
    own_width = residual_in.shape[1]
    attended_full = gathered_copies(attended, "tp", 1)
    group_width = local_heads * HEAD_SIZE
    share = jnp.zeros((local_rows, own_width), jnp.float32)
    for group_index in range(tp_count):
        left_part = attended_full[:, group_index * group_width : (group_index + 1) * group_width]
        right_part = weight_cols[group_index * group_width : (group_index + 1) * group_width, :]
        term = jnp.dot(left_part, right_part, preferred_element_type=jnp.float32).astype(
            jnp.bfloat16
        )
        share = share + term.astype(jnp.float32)
    residual_mid = residual_in.astype(jnp.float32) + share
    squares = taken_together(jnp.sum(residual_mid * residual_mid, axis=1), "tp")
    gain_own = lax.dynamic_slice_in_dim(mlp_gain, tp_index * own_width, own_width, 0)
    normed_own = (residual_mid * lax.rsqrt(squares / D + eps)[:, None] * gain_own).astype(
        jnp.bfloat16
    )
    normed = lax.all_gather(normed_own, "tp", axis=1, tiled=True)
    pieces = sent_together((gate_weight, up_weight), "sp", 0, 1)
    gate_out = jnp.dot(normed, pieces[0], preferred_element_type=jnp.float32)
    up_out = jnp.dot(normed, pieces[1], preferred_element_type=jnp.float32)
    hidden = (jax.nn.silu(gate_out) * up_out).astype(jnp.bfloat16)
    down_terms = jnp.dot(
        hidden,
        lax.all_gather(down_weight, "sp", axis=1, tiled=True),
        preferred_element_type=jnp.float32,
    )
    down_share = summed_on_arrival(down_terms.astype(jnp.bfloat16), "tp", 1)
    return (residual_mid + 0.5 * down_share).astype(jnp.bfloat16)


def solution(mesh):
    in_specs = (
        P("sp", "tp"),
        P("sp", "tp"),
        P("sp", None),
        P("sp", None),
        P(),
        P(),
        P("tp", None),
        P(),
        P("sp", "tp"),
        P("sp", "tp"),
        P("tp", "sp"),
    )
    out_specs = P("sp", "tp")
    return jax.shard_map(
        on_device, mesh=mesh, in_specs=in_specs, out_specs=out_specs, check_vma=False
    )
```

profile of v0, /device:TPU:1, one launch (start us, length us, event | category | flops | bytes accessed | tf_op | source)
XLA Modules:
  0.0 336.8 jit_solution(7837900333065985362)
XLA Ops:
  14.6 5.8 %all-to-all-start.1 = ((bf16[128,8,256]{0,2,1:T(8,128)(2,1)}), bf16[128,8,256]{0,2,1:T(8,128)(2,1)S(1)}, u32[]{:S(2)}, u32[]{:S(2)}) async-start(bf16[128,8,256]{0,2,1:T(8,128)(2,1)} %bitcast.9), calls=%async_computation.1 | async-start | bytes 1048576 | tf_op jit(solution)/shard_map/all_to_all | solution.py:100
  21.4 56.8 %all-gather.5.cloned.1.call-done = bf16[12288,256]{1,0:T(8,128)(2,1)} async-done(((bf16[768,256]{1,0:T(8,128)(2,1)}), bf16[12288,256]{1,0:T(8,128)(2,1)}) %all-gather.5.cloned.1.call-update) | async-done | bytes 6291472 | tf_op jit(solution)/shard_map/all_gather | solution.py:21
  78.2 4.7 %fusion.66 = (bf16[12288,128]{1,0:T(8,128)(2,1)}, bf16[12288,128]{1,0:T(8,128)(2,1)}) fusion(bf16[12288,256]{1,0:T(8,128)(2,1)} %all-gather.5.cloned.1.call-done), kind=kLoop, calls=%fused_computation.114 | loop fusion | bytes 12582912 | tf_op jit(solution)/shard_map/split | solution.py:21
  82.9 71.6 %while.18 = (s32[]{:T(128)}, f32[768]{0:T(1024)S(1)}, f32[768]{0:T(1024)S(1)}, f32[768,128]{1,0:T(8,128)S(1)}, bf16[12288,128]{1,0:T(8,128)(2,1)}, /*index=5*/bf...) while((s32[]{:T(128)}, f32[768]{0:T(1024)S(1)}, ...), condition=%wide.region_5.6_spmd.clone, body=%wide.region_2.5_spmd.clone.sunk | while | flops 818188032 | bytes 46121160 | solution.py:146
  82.9 4.7 %multiply_reduce_fusion.3 = (f32[768]{0:T(1024)S(1)}, f32[2048,768]{1,0:T(8,128)}) fusion(bf16[768,128]{1,0:T(8,128)(2,1)S(1)} %get-tuple-element.268, bf16[12288,128]{1,0:T(8,128)(2,1)} %get-tuple-element.267, s32[]{:T(128)S(6)} %select_n.55), kind=kOutput, calls=%fused_computation.1.clone.1 | convolution fusion | flops 405798144 | bytes 7015428 | tf_op jit(solution)/shard_map/while/body/eval_jaxpr/dot_general | solution.py:135
  87.6 4.2 %fusion.80 = f32[768]{0:T(1024)S(1)} fusion(f32[2048,768]{1,0:T(8,128)} %get-tuple-element.238, f32[768]{0:T(1024)S(1)} %select_maximum_fusion.2), kind=kLoop, calls=%fused_computation.3.clone.1 | loop fusion | flops 4717824 | bytes 6297600 | tf_op jit(solution)/shard_map/while/body/eval_jaxpr/reduce_sum | solution.py:140
  95.0 4.7 %multiply_reduce_fusion.3 = (f32[768]{0:T(1024)S(1)}, f32[2048,768]{1,0:T(8,128)}) fusion(bf16[768,128]{1,0:T(8,128)(2,1)S(1)} %get-tuple-element.268, bf16[12288,128]{1,0:T(8,128)(2,1)} %get-tuple-element.267, s32[]{:T(128)S(6)} %select_n.55), kind=kOutput, calls=%fused_computation.1.clone.1 | convolution fusion | flops 405798144 | bytes 7015428 | tf_op jit(solution)/shard_map/while/body/eval_jaxpr/dot_general | solution.py:135
  99.6 4.1 %fusion.80 = f32[768]{0:T(1024)S(1)} fusion(f32[2048,768]{1,0:T(8,128)} %get-tuple-element.238, f32[768]{0:T(1024)S(1)} %select_maximum_fusion.2), kind=kLoop, calls=%fused_computation.3.clone.1 | loop fusion | flops 4717824 | bytes 6297600 | tf_op jit(solution)/shard_map/while/body/eval_jaxpr/reduce_sum | solution.py:140
  106.7 4.7 %multiply_reduce_fusion.3 = (f32[768]{0:T(1024)S(1)}, f32[2048,768]{1,0:T(8,128)}) fusion(bf16[768,128]{1,0:T(8,128)(2,1)S(1)} %get-tuple-element.268, bf16[12288,128]{1,0:T(8,128)(2,1)} %get-tuple-element.267, s32[]{:T(128)S(6)} %select_n.55), kind=kOutput, calls=%fused_computation.1.clone.1 | convolution fusion | flops 405798144 | bytes 7015428 | tf_op jit(solution)/shard_map/while/body/eval_jaxpr/dot_general | solution.py:135
  111.4 4.2 %fusion.80 = f32[768]{0:T(1024)S(1)} fusion(f32[2048,768]{1,0:T(8,128)} %get-tuple-element.238, f32[768]{0:T(1024)S(1)} %select_maximum_fusion.2), kind=kLoop, calls=%fused_computation.3.clone.1 | loop fusion | flops 4717824 | bytes 6297600 | tf_op jit(solution)/shard_map/while/body/eval_jaxpr/reduce_sum | solution.py:140
  118.8 4.7 %multiply_reduce_fusion.3 = (f32[768]{0:T(1024)S(1)}, f32[2048,768]{1,0:T(8,128)}) fusion(bf16[768,128]{1,0:T(8,128)(2,1)S(1)} %get-tuple-element.268, bf16[12288,128]{1,0:T(8,128)(2,1)} %get-tuple-element.267, s32[]{:T(128)S(6)} %select_n.55), kind=kOutput, calls=%fused_computation.1.clone.1 | convolution fusion | flops 405798144 | bytes 7015428 | tf_op jit(solution)/shard_map/while/body/eval_jaxpr/dot_general | solution.py:135
  123.5 4.2 %fusion.80 = f32[768]{0:T(1024)S(1)} fusion(f32[2048,768]{1,0:T(8,128)} %get-tuple-element.238, f32[768]{0:T(1024)S(1)} %select_maximum_fusion.2), kind=kLoop, calls=%fused_computation.3.clone.1 | loop fusion | flops 4717824 | bytes 6297600 | tf_op jit(solution)/shard_map/while/body/eval_jaxpr/reduce_sum | solution.py:140
  130.9 4.7 %multiply_reduce_fusion.3 = (f32[768]{0:T(1024)S(1)}, f32[2048,768]{1,0:T(8,128)}) fusion(bf16[768,128]{1,0:T(8,128)(2,1)S(1)} %get-tuple-element.268, bf16[12288,128]{1,0:T(8,128)(2,1)} %get-tuple-element.267, s32[]{:T(128)S(6)} %select_n.55), kind=kOutput, calls=%fused_computation.1.clone.1 | convolution fusion | flops 405798144 | bytes 7015428 | tf_op jit(solution)/shard_map/while/body/eval_jaxpr/dot_general | solution.py:135
  135.6 4.2 %fusion.80 = f32[768]{0:T(1024)S(1)} fusion(f32[2048,768]{1,0:T(8,128)} %get-tuple-element.238, f32[768]{0:T(1024)S(1)} %select_maximum_fusion.2), kind=kLoop, calls=%fused_computation.3.clone.1 | loop fusion | flops 4717824 | bytes 6297600 | tf_op jit(solution)/shard_map/while/body/eval_jaxpr/reduce_sum | solution.py:140
  142.9 4.7 %multiply_reduce_fusion.3 = (f32[768]{0:T(1024)S(1)}, f32[2048,768]{1,0:T(8,128)}) fusion(bf16[768,128]{1,0:T(8,128)(2,1)S(1)} %get-tuple-element.268, bf16[12288,128]{1,0:T(8,128)(2,1)} %get-tuple-element.267, s32[]{:T(128)S(6)} %select_n.55), kind=kOutput, calls=%fused_computation.1.clone.1 | convolution fusion | flops 405798144 | bytes 7015428 | tf_op jit(solution)/shard_map/while/body/eval_jaxpr/dot_general | solution.py:135
  147.5 4.0 %fusion.80 = f32[768]{0:T(1024)S(1)} fusion(f32[2048,768]{1,0:T(8,128)} %get-tuple-element.238, f32[768]{0:T(1024)S(1)} %select_maximum_fusion.2), kind=kLoop, calls=%fused_computation.3.clone.1 | loop fusion | flops 4717824 | bytes 6297600 | tf_op jit(solution)/shard_map/while/body/eval_jaxpr/reduce_sum | solution.py:140
  156.2 5.2 %all-to-all-start = ((bf16[8,768,128]{1,2,0:T(8,128)(2,1)}), bf16[8,768,128]{1,2,0:T(8,128)(2,1)S(1)}, u32[]{:S(2)}, u32[]{:S(2)}) async-start(bf16[8,768,128]{1,2,0:T(8,128)(2,1)} %broadcast_in_dim.17), calls=%async_computation | async-start | bytes 3145728 | tf_op jit(solution)/shard_map/all_to_all | solution.py:32
  163.3 18.7 %all-to-all-done = bf16[8,768,128]{1,2,0:T(8,128)(2,1)S(1)} async-done(((bf16[8,768,128]{1,2,0:T(8,128)(2,1)}), bf16[8,768,128]{1,2,0:T(8,128)(2,1)S(1)}, u32[]{:S(2)}, u32[]{:S(2)}) %all-to-all-start) | async-done | bytes 1572896 | tf_op jit(solution)/shard_map/all_to_all | solution.py:32
  184.9 4.2 %all-to-all-start.2 = ((f32[8,1,768]{2,1,0:T(1,128)}), f32[8,1,768]{2,1,0:T(1,128)S(1)}, u32[]{:S(2)}, u32[]{:S(2)}) async-start(f32[8,1,768]{2,1,0:T(1,128)} %broadcast_in_dim.18), calls=%async_computation.2 | async-start | bytes 49152 | tf_op jit(solution)/shard_map/all_to_all | solution.py:32
  195.3 24.9 %all-gather.7.cloned.1.call-done = bf16[768,2048]{0,1:T(8,128)(2,1)} async-done(((bf16[768,256]{0,1:T(8,128)(2,1)}), bf16[768,2048]{0,1:T(8,128)(2,1)}) %all-gather.7.cloned.1.call-update) | async-done | bytes 3145744 | tf_op jit(solution)/shard_map/all_gather | solution.py:168
  220.2 5.2 %fusion.16 = f32[768,704]{0,1:T(8,128)S(1)} fusion(bf16[768,2048]{0,1:T(8,128)(2,1)} %all-gather.7.cloned.1.call-done, bf16[2048,1408]{0,1:T(8,128)(2,1)} %all-gather.9.cloned.1.call-done), kind=kOutput, calls=%fused_computation.22 | convolution fusion | flops 2214592512 | bytes 8192000 | tf_op jit(solution)/shard_map/dot_general | solution.py:170
  225.4 45.8 %all-gather.11.cloned.1.call-done = bf16[704,2048]{1,0:T(8,128)(2,1)} async-done(((bf16[704,128]{1,0:T(8,128)(2,1)}), bf16[704,2048]{1,0:T(8,128)(2,1)}) %all-gather.11.cloned.1.call-update) | async-done | bytes 2883600 | tf_op jit(solution)/shard_map/all_gather | solution.py:175
  271.2 11.7 %convolution_convert_fusion = bf16[768,2048]{1,0:T(8,128)(2,1)} fusion(bf16[704,2048]{1,0:T(8,128)(2,1)} %all-gather.11.cloned.1.call-done, f32[768,704]{0,1:T(8,128)S(1)} %fusion.16, bf16[768,2048]{0,1:T(8,128)(2,1)} %all-gather.7.cloned.1.call-done, bf16[2048,1408]{0,1:T(8,128)(2,1)} %all-gather.9.cloned.1.call-done), kind=kOutput, calls=%fused_computation.18 | convolution fusion | flops 4434001920 | bytes 14221312 | tf_op jit(solution)/shard_map/dot_general | solution.py:173
  285.0 43.5 %all_to_all.32 = bf16[8,768,256]{2,1,0:T(8,128)(2,1)S(1)} all-to-all(bf16[8,768,256]{2,1,0:T(8,128)(2,1)S(1)} %bitcast.66), channel_id=1, replica_groups=mesh['sp'=16,'tp'=8] {'tp'}, dimensions={0} | all-to-all | bytes 6291456 | tf_op jit(solution)/shard_map/all_to_all | solution.py:52
  (98 shorter events, 43.8 us)
Async XLA Ops:
  6.5 2.4 copy-start
  6.5 71.7 %all-gather.5.cloned.1.call-start = ((), (), s32[]{:S(2)}) async-start(), calls=%async_computation.4 | async-start | bytes 6684672 | tf_op jit(solution)/shard_map/all_gather | solution.py:21
  10.5 3.1 copy-start.3
  12.3 8.1 %copy-start.4 = (bf16[128,704]{0,1:T(8,128)(2,1)S(1)}, bf16[128,704]{0,1:T(8,128)(2,1)}, u32[]{:S(2)}) copy-start(bf16[128,704]{0,1:T(8,128)(2,1)} %param.22) | copy-start | bytes 540676
  12.3 8.1 %copy-start.5 = (bf16[128,704]{0,1:T(8,128)(2,1)S(1)}, bf16[128,704]{0,1:T(8,128)(2,1)}, u32[]{:S(2)}) copy-start(bf16[128,704]{0,1:T(8,128)(2,1)} %param.21) | copy-start | bytes 540676
  14.6 140.2 %all-to-all-start.1 = ((bf16[128,8,256]{0,2,1:T(8,128)(2,1)}), bf16[128,8,256]{0,2,1:T(8,128)(2,1)S(1)}, u32[]{:S(2)}, u32[]{:S(2)}) async-start(bf16[128,8,256]{0,2,1:T(8,128)(2,1)} %bitcast.9), calls=%async_computation.1 | async-start | bytes 1048576 | tf_op jit(solution)/shard_map/all_to_all | solution.py:100
  20.4 174.9 %all-gather.9.cloned.1.call-start = ((), (), s32[]{:S(2)}) async-start(), calls=%async_computation.6 | async-start | bytes 6127616 | tf_op jit(solution)/shard_map/all_gather | solution.py:21
  87.6 5.0 %copy-start.1 = (f32[2048,768]{1,0:T(8,128)S(1)}, f32[2048,768]{1,0:T(8,128)}, u32[]{:S(2)}) copy-start(f32[2048,768]{1,0:T(8,128)} %get-tuple-element.238) | copy-start | bytes 18874372 | tf_op jit(solution)/shard_map/while
  99.6 4.7 %copy-start.1 = (f32[2048,768]{1,0:T(8,128)S(1)}, f32[2048,768]{1,0:T(8,128)}, u32[]{:S(2)}) copy-start(f32[2048,768]{1,0:T(8,128)} %get-tuple-element.238) | copy-start | bytes 18874372 | tf_op jit(solution)/shard_map/while
  111.4 5.0 %copy-start.1 = (f32[2048,768]{1,0:T(8,128)S(1)}, f32[2048,768]{1,0:T(8,128)}, u32[]{:S(2)}) copy-start(f32[2048,768]{1,0:T(8,128)} %get-tuple-element.238) | copy-start | bytes 18874372 | tf_op jit(solution)/shard_map/while
  123.5 5.0 %copy-start.1 = (f32[2048,768]{1,0:T(8,128)S(1)}, f32[2048,768]{1,0:T(8,128)}, u32[]{:S(2)}) copy-start(f32[2048,768]{1,0:T(8,128)} %get-tuple-element.238) | copy-start | bytes 18874372 | tf_op jit(solution)/shard_map/while
  135.6 4.9 %copy-start.1 = (f32[2048,768]{1,0:T(8,128)S(1)}, f32[2048,768]{1,0:T(8,128)}, u32[]{:S(2)}) copy-start(f32[2048,768]{1,0:T(8,128)} %get-tuple-element.238) | copy-start | bytes 18874372 | tf_op jit(solution)/shard_map/while
  147.5 4.6 %copy-start.1 = (f32[2048,768]{1,0:T(8,128)S(1)}, f32[2048,768]{1,0:T(8,128)}, u32[]{:S(2)}) copy-start(f32[2048,768]{1,0:T(8,128)} %get-tuple-element.238) | copy-start | bytes 18874372 | tf_op jit(solution)/shard_map/while
  156.2 25.8 %all-to-all-start = ((bf16[8,768,128]{1,2,0:T(8,128)(2,1)}), bf16[8,768,128]{1,2,0:T(8,128)(2,1)S(1)}, u32[]{:S(2)}, u32[]{:S(2)}) async-start(bf16[8,768,128]{1,2,0:T(8,128)(2,1)} %broadcast_in_dim.17), calls=%async_computation | async-start | bytes 3145728 | tf_op jit(solution)/shard_map/all_to_all | solution.py:32
  183.0 1.0 copy-start.2
  184.9 8.9 %all-to-all-start.2 = ((f32[8,1,768]{2,1,0:T(1,128)}), f32[8,1,768]{2,1,0:T(1,128)S(1)}, u32[]{:S(2)}, u32[]{:S(2)}) async-start(f32[8,1,768]{2,1,0:T(1,128)} %broadcast_in_dim.18), calls=%async_computation.2 | async-start | bytes 49152 | tf_op jit(solution)/shard_map/all_to_all | solution.py:32
  189.1 31.1 %all-gather.7.cloned.1.call-start = ((), (), s32[]{:S(2)}) async-start(), calls=%async_computation.5 | async-start | bytes 3538944 | tf_op jit(solution)/shard_map/all_gather | solution.py:168
  194.7 76.4 %all-gather.11.cloned.1.call-start = ((), (), s32[]{:S(2)}) async-start(), calls=%async_computation.7 | async-start | bytes 3063808 | tf_op jit(solution)/shard_map/all_gather | solution.py:175
Sparse Core Ops, SparseCore 0:
  13.7 64.4 all-gather.4
  80.3 62.8 all-gather.8
  194.9 25.3 all-gather.6
  222.2 48.9 all-gather.10
where the time goes:
time: 338 us; the launch traced here: 337 us
  waiting for transfers between devices  151 us (45%)
  matrix products  61.1 us (18%)
  blocking collectives  43.5 us (13%)
  other arithmetic  34.3 us (10%)
  local copies, waits for them, and re-layouts  18.2 us (5%)
  starting transfers between devices  15.5 us (5%)
  between operations  13.4 us (4%)
    all_gather x2, waiting for transfers between devices, sent_together(): lax.all_gather(both, axis, axis=dim, tiled=True)  56.8 us
    all_gather x1, waiting for transfers between devices, on_device(): lax.all_gather(down_weight, 'sp', axis=1, tiled=True)  45.8 us
    all_to_all x1, blocking collectives, summed_on_arrival(): lax.all_to_all(tiles, axis, split_axis=0, concat_axis=0, tiled=True)  43.5 us
    dot_general x6, matrix products, one_block(): jnp.dot(query_matrix, block_keys.T, preferred_element_type=jnp.float32)  28 us
    all_gather x1, waiting for transfers between devices, on_device(): normed = lax.all_gather(normed_own, 'tp', axis=1, tiled=True)  24.9 us
    reduce_sum x6, other arithmetic, one_block(): running_sum = running_sum * factor + jnp.sum(weights, axis=1)  24.8 us
    all_to_all x2, waiting for transfers between devices, sent_to_all(): lax.all_to_all(jnp.broadcast_to(x[None], (size, *x.shape)), axis, 0, 0, t...  22.6 us
    dot_general x6, matrix products, one_block(): jnp.dot(weights.astype(jnp.bfloat16), block_values, preferred_element_typ...  14.2 us
  transfers between devices with their start and end apart: 7, of which 5 were waited for; matrix products, arithmetic and copies ran while one was open for 26% of the time, Pallas kernels for 0%

commit v1 on v0

--- a/solution.py
+++ b/solution.py
@@ -10,6 +10,12 @@
 GRID = 64
 eps = 1e-06
 rotary_base = 10000.0
+
+
+def stack_and_merge(x, axis, dim):
+    parts = lax.all_gather(x, axis, axis=0, tiled=False)
+    full = jnp.concatenate(parts, axis=dim)
+    return full
 
 
 def sent_together(arrays, axis, dim, along):
@@ -171,9 +177,7 @@
     up_out = jnp.dot(normed, pieces[1], preferred_element_type=jnp.float32)
     hidden = (jax.nn.silu(gate_out) * up_out).astype(jnp.bfloat16)
     down_terms = jnp.dot(
-        hidden,
-        lax.all_gather(down_weight, "sp", axis=1, tiled=True),
-        preferred_element_type=jnp.float32,
+        hidden, stack_and_merge(down_weight, "sp", 1), preferred_element_type=jnp.float32
     )
     down_share = summed_on_arrival(down_terms.astype(jnp.bfloat16), "tp", 1)
     return (residual_mid + 0.5 * down_share).astype(jnp.bfloat16)

time: 338 us -> 291 us (0.86)
  waiting for transfers between devices: 151 us -> 102 us
  local copies, waits for them, and re-layouts: 18.2 us -> 23.1 us
    all_gather x1, waiting for transfers between devices: 45.8 us -> 0.02 us  [stack_and_merge(): parts = lax.all_gather(x, axis, axis=0, tiled=False)]
    all_gather x0 -> x1, local copies, waits for them, and re-layouts: none -> 5.27 us  [stack_and_merge(): parts = lax.all_gather(x, axis, axis=0, tiled=False)]
  transfers between devices with their start and end apart: 7 -> 7, of which waited for: 5 -> 4; matrix products, arithmetic and copies ran while one was open for 26% -> 30% of each run, Pallas kernels for 0% -> 0%
where the time goes in v1:
time: 291 us; the launch traced here: 289 us
  waiting for transfers between devices  102 us (35%)
  matrix products  61.3 us (21%)
  blocking collectives  40.4 us (14%)
  other arithmetic  33.7 us (12%)
  local copies, waits for them, and re-layouts  23.1 us (8%)
  starting transfers between devices  15.2 us (5%)
  between operations  13.4 us (5%)
    all_gather x2, waiting for transfers between devices, sent_together(): lax.all_gather(both, axis, axis=dim, tiled=True)  56.1 us
    all_to_all x1, blocking collectives, summed_on_arrival(): lax.all_to_all(tiles, axis, split_axis=0, concat_axis=0, tiled=True)  40.4 us
    dot_general x6, matrix products, one_block(): jnp.dot(query_matrix, block_keys.T, preferred_element_type=jnp.float32)  28 us
    reduce_sum x6, other arithmetic, one_block(): running_sum = running_sum * factor + jnp.sum(weights, axis=1)  24.3 us
    all_to_all x2, waiting for transfers between devices, sent_to_all(): lax.all_to_all(jnp.broadcast_to(x[None], (size, *x.shape)), axis, 0, 0, t...  22.7 us
    all_gather x1, waiting for transfers between devices, on_device(): normed = lax.all_gather(normed_own, 'tp', axis=1, tiled=True)  22.6 us
    dot_general x6, matrix products, one_block(): jnp.dot(weights.astype(jnp.bfloat16), block_values, preferred_element_typ...  14.3 us
    dot_general x1, matrix products, on_device(): jnp.dot(hidden, stack_and_merge(down_weight, 'sp', 1), preferred_element_...  11.8 us
  transfers between devices with their start and end apart: 7, of which 4 were waited for; matrix products, arithmetic and copies ran while one was open for 30% of the time, Pallas kernels for 0%

profile of v1, /device:TPU:1, one launch (start us, length us, event | category | flops | bytes accessed | tf_op | source)
XLA Modules:
  0.0 289.5 jit_solution(3912065818291232085)
XLA Ops:
  15.4 5.8 %all-to-all-start.1 = ((bf16[128,8,256]{0,2,1:T(8,128)(2,1)}), bf16[128,8,256]{0,2,1:T(8,128)(2,1)S(1)}, u32[]{:S(2)}, u32[]{:S(2)}) async-start(bf16[128,8,256]{0,2,1:T(8,128)(2,1)} %bitcast.9), calls=%async_computation.1 | async-start | bytes 1048576 | tf_op jit(solution)/shard_map/all_to_all | solution.py:106
  22.2 56.0 %all-gather.6.cloned.1.call-done = bf16[12288,256]{1,0:T(8,128)(2,1)} async-done(((bf16[768,256]{1,0:T(8,128)(2,1)}), bf16[12288,256]{1,0:T(8,128)(2,1)}) %all-gather.6.cloned.1.call-update) | async-done | bytes 6291472 | tf_op jit(solution)/shard_map/all_gather | solution.py:27
  78.2 4.7 %fusion.68 = (bf16[12288,128]{1,0:T(8,128)(2,1)}, bf16[12288,128]{1,0:T(8,128)(2,1)}) fusion(bf16[12288,256]{1,0:T(8,128)(2,1)} %all-gather.6.cloned.1.call-done), kind=kLoop, calls=%fused_computation.116 | loop fusion | bytes 12582912 | tf_op jit(solution)/shard_map/split | solution.py:27
  82.9 70.7 %while.18 = (s32[]{:T(128)}, f32[768]{0:T(1024)S(1)}, f32[768]{0:T(1024)S(1)}, f32[768,128]{1,0:T(8,128)S(1)}, bf16[12288,128]{1,0:T(8,128)(2,1)}, /*index=5*/bf...) while((s32[]{:T(128)}, f32[768]{0:T(1024)S(1)}, ...), condition=%wide.region_5.6_spmd.clone, body=%wide.region_2.5_spmd.clone.sunk | while | flops 818188032 | bytes 46121160 | solution.py:152
  82.9 4.7 %multiply_reduce_fusion.3 = (f32[768]{0:T(1024)S(1)}, f32[2048,768]{1,0:T(8,128)}) fusion(bf16[768,128]{1,0:T(8,128)(2,1)S(1)} %get-tuple-element.268, bf16[12288,128]{1,0:T(8,128)(2,1)} %get-tuple-element.267, s32[]{:T(128)S(6)} %select_n.55), kind=kOutput, calls=%fused_computation.1.clone.1 | convolution fusion | flops 405798144 | bytes 7015428 | tf_op jit(solution)/shard_map/while/body/eval_jaxpr/dot_general | solution.py:141
  87.6 4.1 %fusion.81 = f32[768]{0:T(1024)S(1)} fusion(f32[2048,768]{1,0:T(8,128)} %get-tuple-element.238, f32[768]{0:T(1024)S(1)} %select_maximum_fusion.2), kind=kLoop, calls=%fused_computation.3.clone.1 | loop fusion | flops 4717824 | bytes 6297600 | tf_op jit(solution)/shard_map/while/body/eval_jaxpr/reduce_sum | solution.py:146
  94.8 4.7 %multiply_reduce_fusion.3 = (f32[768]{0:T(1024)S(1)}, f32[2048,768]{1,0:T(8,128)}) fusion(bf16[768,128]{1,0:T(8,128)(2,1)S(1)} %get-tuple-element.268, bf16[12288,128]{1,0:T(8,128)(2,1)} %get-tuple-element.267, s32[]{:T(128)S(6)} %select_n.55), kind=kOutput, calls=%fused_computation.1.clone.1 | convolution fusion | flops 405798144 | bytes 7015428 | tf_op jit(solution)/shard_map/while/body/eval_jaxpr/dot_general | solution.py:141
  99.5 4.0 %fusion.81 = f32[768]{0:T(1024)S(1)} fusion(f32[2048,768]{1,0:T(8,128)} %get-tuple-element.238, f32[768]{0:T(1024)S(1)} %select_maximum_fusion.2), kind=kLoop, calls=%fused_computation.3.clone.1 | loop fusion | flops 4717824 | bytes 6297600 | tf_op jit(solution)/shard_map/while/body/eval_jaxpr/reduce_sum | solution.py:146
  106.5 4.7 %multiply_reduce_fusion.3 = (f32[768]{0:T(1024)S(1)}, f32[2048,768]{1,0:T(8,128)}) fusion(bf16[768,128]{1,0:T(8,128)(2,1)S(1)} %get-tuple-element.268, bf16[12288,128]{1,0:T(8,128)(2,1)} %get-tuple-element.267, s32[]{:T(128)S(6)} %select_n.55), kind=kOutput, calls=%fused_computation.1.clone.1 | convolution fusion | flops 405798144 | bytes 7015428 | tf_op jit(solution)/shard_map/while/body/eval_jaxpr/dot_general | solution.py:141
  111.2 4.0 %fusion.81 = f32[768]{0:T(1024)S(1)} fusion(f32[2048,768]{1,0:T(8,128)} %get-tuple-element.238, f32[768]{0:T(1024)S(1)} %select_maximum_fusion.2), kind=kLoop, calls=%fused_computation.3.clone.1 | loop fusion | flops 4717824 | bytes 6297600 | tf_op jit(solution)/shard_map/while/body/eval_jaxpr/reduce_sum | solution.py:146
  118.2 4.7 %multiply_reduce_fusion.3 = (f32[768]{0:T(1024)S(1)}, f32[2048,768]{1,0:T(8,128)}) fusion(bf16[768,128]{1,0:T(8,128)(2,1)S(1)} %get-tuple-element.268, bf16[12288,128]{1,0:T(8,128)(2,1)} %get-tuple-element.267, s32[]{:T(128)S(6)} %select_n.55), kind=kOutput, calls=%fused_computation.1.clone.1 | convolution fusion | flops 405798144 | bytes 7015428 | tf_op jit(solution)/shard_map/while/body/eval_jaxpr/dot_general | solution.py:141
  122.9 4.0 %fusion.81 = f32[768]{0:T(1024)S(1)} fusion(f32[2048,768]{1,0:T(8,128)} %get-tuple-element.238, f32[768]{0:T(1024)S(1)} %select_maximum_fusion.2), kind=kLoop, calls=%fused_computation.3.clone.1 | loop fusion | flops 4717824 | bytes 6297600 | tf_op jit(solution)/shard_map/while/body/eval_jaxpr/reduce_sum | solution.py:146
  129.9 4.7 %multiply_reduce_fusion.3 = (f32[768]{0:T(1024)S(1)}, f32[2048,768]{1,0:T(8,128)}) fusion(bf16[768,128]{1,0:T(8,128)(2,1)S(1)} %get-tuple-element.268, bf16[12288,128]{1,0:T(8,128)(2,1)} %get-tuple-element.267, s32[]{:T(128)S(6)} %select_n.55), kind=kOutput, calls=%fused_computation.1.clone.1 | convolution fusion | flops 405798144 | bytes 7015428 | tf_op jit(solution)/shard_map/while/body/eval_jaxpr/dot_general | solution.py:141
  134.6 4.0 %fusion.81 = f32[768]{0:T(1024)S(1)} fusion(f32[2048,768]{1,0:T(8,128)} %get-tuple-element.238, f32[768]{0:T(1024)S(1)} %select_maximum_fusion.2), kind=kLoop, calls=%fused_computation.3.clone.1 | loop fusion | flops 4717824 | bytes 6297600 | tf_op jit(solution)/shard_map/while/body/eval_jaxpr/reduce_sum | solution.py:146
  141.8 4.7 %multiply_reduce_fusion.3 = (f32[768]{0:T(1024)S(1)}, f32[2048,768]{1,0:T(8,128)}) fusion(bf16[768,128]{1,0:T(8,128)(2,1)S(1)} %get-tuple-element.268, bf16[12288,128]{1,0:T(8,128)(2,1)} %get-tuple-element.267, s32[]{:T(128)S(6)} %select_n.55), kind=kOutput, calls=%fused_computation.1.clone.1 | convolution fusion | flops 405798144 | bytes 7015428 | tf_op jit(solution)/shard_map/while/body/eval_jaxpr/dot_general | solution.py:141
  146.5 4.1 %fusion.81 = f32[768]{0:T(1024)S(1)} fusion(f32[2048,768]{1,0:T(8,128)} %get-tuple-element.238, f32[768]{0:T(1024)S(1)} %select_maximum_fusion.2), kind=kLoop, calls=%fused_computation.3.clone.1 | loop fusion | flops 4717824 | bytes 6297600 | tf_op jit(solution)/shard_map/while/body/eval_jaxpr/reduce_sum | solution.py:146
  155.2 5.1 %all-to-all-start = ((bf16[8,768,128]{1,2,0:T(8,128)(2,1)}), bf16[8,768,128]{1,2,0:T(8,128)(2,1)S(1)}, u32[]{:S(2)}, u32[]{:S(2)}) async-start(bf16[8,768,128]{1,2,0:T(8,128)(2,1)} %broadcast_in_dim.17), calls=%async_computation | async-start | bytes 3145728 | tf_op jit(solution)/shard_map/all_to_all | solution.py:38
  162.3 18.7 %all-to-all-done = bf16[8,768,128]{1,2,0:T(8,128)(2,1)S(1)} async-done(((bf16[8,768,128]{1,2,0:T(8,128)(2,1)}), bf16[8,768,128]{1,2,0:T(8,128)(2,1)S(1)}, u32[]{:S(2)}, u32[]{:S(2)}) %all-to-all-start) | async-done | bytes 1572896 | tf_op jit(solution)/shard_map/all_to_all | solution.py:38
  183.9 4.2 %all-to-all-start.2 = ((f32[8,1,768]{2,1,0:T(1,128)}), f32[8,1,768]{2,1,0:T(1,128)S(1)}, u32[]{:S(2)}, u32[]{:S(2)}) async-start(f32[8,1,768]{2,1,0:T(1,128)} %broadcast_in_dim.18), calls=%async_computation.2 | async-start | bytes 49152 | tf_op jit(solution)/shard_map/all_to_all | solution.py:38
  193.8 5.3 %copy.75 = bf16[16,704,128]{2,0,1:T(8,128)(2,1)} copy(bf16[16,704,128]{2,1,0:T(8,128)(2,1)} %bitcast.81) | data formatting | bytes 5767168 | tf_op jit(solution)/shard_map/all_gather | solution.py:16
  199.1 22.6 %all-gather.8.cloned.1.call-done = bf16[768,2048]{0,1:T(8,128)(2,1)} async-done(((bf16[768,256]{0,1:T(8,128)(2,1)}), bf16[768,2048]{0,1:T(8,128)(2,1)}) %all-gather.8.cloned.1.call-update) | async-done | bytes 3145744 | tf_op jit(solution)/shard_map/all_gather | solution.py:174
  221.7 5.2 %fusion.18 = f32[768,704]{0,1:T(8,128)S(1)} fusion(bf16[768,2048]{0,1:T(8,128)(2,1)} %all-gather.8.cloned.1.call-done, bf16[2048,1408]{0,1:T(8,128)(2,1)} %all-gather.10.cloned.1.call-done), kind=kOutput, calls=%fused_computation.24 | convolution fusion | flops 2214592512 | bytes 8192000 | tf_op jit(solution)/shard_map/dot_general | solution.py:176
  226.9 11.8 %convolution_convert_fusion = bf16[768,2048]{1,0:T(8,128)(2,1)} fusion(bf16[88,8,16,128]{3,2,1,0:T(8,128)(2,1)} %bitcast.82, f32[768,704]{0,1:T(8,128)S(1)} %fusion.18, bf16[768,2048]{0,1:T(8,128)(2,1)} %all-gather.8.cloned.1.call-done, bf16[2048,1408]{0,1:T(8,128)(2,1)} %all-gather.10.cloned.1.call-done), kind=kOutput, calls=%fused_computation.18 | convolution fusion | flops 4434001920 | bytes 14221312 | tf_op jit(solution)/shard_map/dot_general | solution.py:179
  240.8 40.4 %all_to_all.32 = bf16[8,768,256]{2,1,0:T(8,128)(2,1)S(1)} all-to-all(bf16[8,768,256]{2,1,0:T(8,128)(2,1)S(1)} %bitcast.71), channel_id=1, replica_groups=mesh['sp'=16,'tp'=8] {'tp'}, dimensions={0} | all-to-all | bytes 6291456 | tf_op jit(solution)/shard_map/all_to_all | solution.py:58
  (99 shorter events, 43.7 us)
Async XLA Ops:
  6.5 2.4 copy-start
  6.5 71.7 %all-gather.6.cloned.1.call-start = ((), (), s32[]{:S(2)}) async-start(), calls=%async_computation.4 | async-start | bytes 6684672 | tf_op jit(solution)/shard_map/all_gather | solution.py:27
  10.5 3.8 %copy-start.3 = (bf16[128,2048]{1,0:T(8,128)(2,1)S(1)}, bf16[128,2048]{1,0:T(8,128)(2,1)}, u32[]{:S(2)}) copy-start(bf16[128,2048]{1,0:T(8,128)(2,1)} %param.19) | copy-start | bytes 1572868
  12.3 8.9 %copy-start.4 = (bf16[128,704]{0,1:T(8,128)(2,1)S(1)}, bf16[128,704]{0,1:T(8,128)(2,1)}, u32[]{:S(2)}) copy-start(bf16[128,704]{0,1:T(8,128)(2,1)} %param.22) | copy-start | bytes 540676
  12.3 8.9 %copy-start.5 = (bf16[128,704]{0,1:T(8,128)(2,1)S(1)}, bf16[128,704]{0,1:T(8,128)(2,1)}, u32[]{:S(2)}) copy-start(bf16[128,704]{0,1:T(8,128)(2,1)} %param.21) | copy-start | bytes 540676
  13.6 180.2 %all-gather.12.cloned.1.call-start = ((), (), s32[]{:S(2)}) async-start(), calls=%async_computation.7 | async-start | bytes 3063808 | tf_op jit(solution)/shard_map/all_gather | solution.py:16
  15.4 138.5 %all-to-all-start.1 = ((bf16[128,8,256]{0,2,1:T(8,128)(2,1)}), bf16[128,8,256]{0,2,1:T(8,128)(2,1)S(1)}, u32[]{:S(2)}, u32[]{:S(2)}) async-start(bf16[128,8,256]{0,2,1:T(8,128)(2,1)} %bitcast.9), calls=%async_computation.1 | async-start | bytes 1048576 | tf_op jit(solution)/shard_map/all_to_all | solution.py:106
  21.2 177.9 %all-gather.10.cloned.1.call-start = ((), (), s32[]{:S(2)}) async-start(), calls=%async_computation.6 | async-start | bytes 6127616 | tf_op jit(solution)/shard_map/all_gather | solution.py:27
  87.6 4.8 %copy-start.1 = (f32[2048,768]{1,0:T(8,128)S(1)}, f32[2048,768]{1,0:T(8,128)}, u32[]{:S(2)}) copy-start(f32[2048,768]{1,0:T(8,128)} %get-tuple-element.238) | copy-start | bytes 18874372 | tf_op jit(solution)/shard_map/while
  99.5 4.6 %copy-start.1 = (f32[2048,768]{1,0:T(8,128)S(1)}, f32[2048,768]{1,0:T(8,128)}, u32[]{:S(2)}) copy-start(f32[2048,768]{1,0:T(8,128)} %get-tuple-element.238) | copy-start | bytes 18874372 | tf_op jit(solution)/shard_map/while
  111.2 4.6 %copy-start.1 = (f32[2048,768]{1,0:T(8,128)S(1)}, f32[2048,768]{1,0:T(8,128)}, u32[]{:S(2)}) copy-start(f32[2048,768]{1,0:T(8,128)} %get-tuple-element.238) | copy-start | bytes 18874372 | tf_op jit(solution)/shard_map/while
  122.9 4.6 %copy-start.1 = (f32[2048,768]{1,0:T(8,128)S(1)}, f32[2048,768]{1,0:T(8,128)}, u32[]{:S(2)}) copy-start(f32[2048,768]{1,0:T(8,128)} %get-tuple-element.238) | copy-start | bytes 18874372 | tf_op jit(solution)/shard_map/while
  134.6 4.8 %copy-start.1 = (f32[2048,768]{1,0:T(8,128)S(1)}, f32[2048,768]{1,0:T(8,128)}, u32[]{:S(2)}) copy-start(f32[2048,768]{1,0:T(8,128)} %get-tuple-element.238) | copy-start | bytes 18874372 | tf_op jit(solution)/shard_map/while
  146.5 4.7 %copy-start.1 = (f32[2048,768]{1,0:T(8,128)S(1)}, f32[2048,768]{1,0:T(8,128)}, u32[]{:S(2)}) copy-start(f32[2048,768]{1,0:T(8,128)} %get-tuple-element.238) | copy-start | bytes 18874372 | tf_op jit(solution)/shard_map/while
  155.2 25.7 %all-to-all-start = ((bf16[8,768,128]{1,2,0:T(8,128)(2,1)}), bf16[8,768,128]{1,2,0:T(8,128)(2,1)S(1)}, u32[]{:S(2)}, u32[]{:S(2)}) async-start(bf16[8,768,128]{1,2,0:T(8,128)(2,1)} %broadcast_in_dim.17), calls=%async_computation | async-start | bytes 3145728 | tf_op jit(solution)/shard_map/all_to_all | solution.py:38
  181.9 1.0 copy-start.2
  183.9 9.0 %all-to-all-start.2 = ((f32[8,1,768]{2,1,0:T(1,128)}), f32[8,1,768]{2,1,0:T(1,128)S(1)}, u32[]{:S(2)}, u32[]{:S(2)}) async-start(f32[8,1,768]{2,1,0:T(1,128)} %broadcast_in_dim.18), calls=%async_computation.2 | async-start | bytes 49152 | tf_op jit(solution)/shard_map/all_to_all | solution.py:38
  188.1 33.6 %all-gather.8.cloned.1.call-start = ((), (), s32[]{:S(2)}) async-start(), calls=%async_computation.5 | async-start | bytes 3538944 | tf_op jit(solution)/shard_map/all_gather | solution.py:174
Sparse Core Ops, SparseCore 0:
  13.7 64.4 all-gather.5
  80.3 46.0 all-gather.11
  128.6 62.8 all-gather.9
  193.9 27.7 all-gather.7
